TPU v7x, 512 devices: a whole 4x4x16 slice. The times are simulated.
512 devices in a mesh: ep: 16 (over y, x), tp: 32 (over z, core).
Axes of the slice: x: 4, y: 4, z: 16, core: 2. Of those that a mesh axis runs over, the one named last changes fastest.
Arguments:
- tokens: bfloat16 [2048, 4096], P('ep', 'tp'), may hold values from -16 to 16
- routing: int32 [2048, 4], P('ep'), may hold values from 0 to 31, all different within a row; in each aligned block of 128 rows (0 to 127, 128 to 255, ...) at most 32 rows name the same one
- gate_weights: float32 [2048, 4], P('ep'), may hold values from 0.1 to 1
- w_gate: bfloat16 [32, 1024, 4096], P('ep', 'tp'), may hold values from -0.09375 to 0.09375
- w_up: bfloat16 [32, 1024, 4096], P('ep', 'tp'), may hold values from -0.09375 to 0.09375
- w_down: bfloat16 [32, 1024, 4096], P('ep', None, 'tp'), may hold values from -2 to 2
- out_gain: float32 [4096], P('tp'), may hold values from 0.1 to 1.9
Outputs:
- mixed: bfloat16 [2048, 4096], P('ep', 'tp')
Inputs may be any that keep to these rules, and one draw needn't show every extreme that they name: `routing`: in each aligned block of 128 rows (the tokens of one index of ep) no expert is named by more than 32 entries, and in every draw some expert is named by exactly 32 entries of some block. The 4 entries of a row differ.
All inputs are finite; a program needn't handle non-finite values.
Results may differ from a plain program's by a relative error of at most 0.0057.
Values may be sent and summed in bfloat16 or wider, within the bound.
A program may use at most 64 MiB of HBM per device.

v0:
```python
import jax
import jax.numpy as jnp
from jax import lax
from jax.sharding import PartitionSpec as P

D = 4096
TOPK = 4
EXP_DEV = 2


norm_eps = 1e-05


def from_everyone(value, axis):
    length = lax.axis_size(axis)
    return lax.all_to_all(
        jnp.broadcast_to(value[None], (length, *value.shape)), axis, 0, 0, tiled=True
    )


def taken_together(value, axis):
    return from_everyone(value, axis).sum(axis=0)


def body(tokens, routing, gate_weights, w_gate, w_up, w_down, out_gain):
    ep_count = lax.axis_size("ep")
    tok_rows = tokens.shape[0]
    width_part = tokens.shape[1]
    experts = EXP_DEV * ep_count
    slot_count = 2 * tok_rows * TOPK // experts
    span_rows = ep_count * slot_count
    total_slots = EXP_DEV * span_rows
    flat_route = routing.reshape(-1)
    expert_ids = jnp.arange(experts, dtype=jnp.int32)
    hit_table = (flat_route[:, None] == expert_ids[None, :]).astype(jnp.int32)
    running = jnp.cumsum(hit_table, axis=0) - hit_table
    slot_rank = jnp.sum(running * hit_table, axis=1)
    slot_target = flat_route % EXP_DEV * span_rows + flat_route // EXP_DEV * slot_count + slot_rank
    entry_targets = slot_target.reshape(tok_rows, TOPK)
    slot_ids = jnp.arange(total_slots, dtype=jnp.int32)
    select_table = jnp.any(entry_targets[None, :, :] == slot_ids[:, None, None], axis=2).astype(
        jnp.bfloat16
    )
    outgoing = jnp.dot(select_table, tokens, preferred_element_type=jnp.float32).astype(
        jnp.bfloat16
    )
    outgoing = outgoing.reshape(EXP_DEV, ep_count, slot_count, width_part)
    arrived = lax.all_to_all(outgoing, "ep", split_axis=1, concat_axis=1, tiled=True).reshape(
        EXP_DEV, span_rows, width_part
    )
    piece_cols = lax.all_gather(arrived, "tp", axis=2, tiled=True)
    gate_sum = jnp.einsum("efn,esn->efs", w_gate, piece_cols, preferred_element_type=jnp.float32)
    up_sum = jnp.einsum("efn,esn->efs", w_up, piece_cols, preferred_element_type=jnp.float32)
    square_sum = jnp.einsum(
        "esn,esn->es", piece_cols, piece_cols, preferred_element_type=jnp.float32
    )
    row_scale = lax.rsqrt(square_sum / D + norm_eps)[:, None, :]
    hidden = (jax.nn.silu(gate_sum * row_scale) * (up_sum * row_scale)).astype(jnp.bfloat16)
    out_part = w_down.shape[2]
    expert_out = jnp.einsum(
        "ens,end->esd",
        lax.all_gather(hidden, "tp", axis=1, tiled=True),
        w_down,
        preferred_element_type=jnp.float32,
    ).astype(jnp.bfloat16)
    returned = lax.all_to_all(
        expert_out.reshape(EXP_DEV, ep_count, slot_count, out_part),
        "ep",
        split_axis=1,
        concat_axis=1,
        tiled=True,
    )
    returned = returned.reshape(total_slots, out_part)
    chosen = returned[slot_target].astype(jnp.float32).reshape(tok_rows, TOPK, out_part)
    combined = jnp.sum(chosen * gate_weights[:, :, None], axis=1)
    square_total = taken_together(jnp.sum(combined * combined, axis=1), "tp")
    final_scale = lax.rsqrt(square_total / D + norm_eps)
    return (combined * final_scale[:, None] * out_gain[None, :]).astype(jnp.bfloat16)


def solution(mesh):
    placed = (
        P("ep", "tp"),
        P("ep", None),
        P("ep", None),
        P("ep", "tp", None),
        P("ep", "tp", None),
        P("ep", None, "tp"),
        P("tp"),
    )
    return jax.shard_map(body, mesh=mesh, in_specs=placed, out_specs=P("ep", "tp"), check_vma=False)
```

profile of v0, /device:TPU:1, one launch (start us, length us, event | category | flops | bytes accessed | tf_op | source)
XLA Modules:
  0.0 253.4 jit_solution(5410838036807146994)
XLA Ops:
  6.5 0.0 copy-start
  6.5 0.0 copy-start.2
  6.5 0.0 all-gather.3.cloned.1.call-start
  6.5 0.9 copy.73
  7.4 0.1 eq.44
  7.5 0.1 eq.40
  7.6 1.2 reduce-window.6
  8.8 0.2 slice_reduce_fusion
  9.1 0.1 fusion.9
  9.2 0.1 reduce_sum.41
  9.3 0.1 copy.76
  9.4 0.7 fusion.13
  10.1 0.4 fusion.1
  10.4 1.0 convolution_convert_fusion.1
  11.5 14.9 %all_to_all.16 = bf16[2,16,32,128]{3,2,0,1:T(8,128)(2,1)S(1)} all-to-all(bf16[2,16,32,128]{3,2,0,1:T(8,128)(2,1)S(1)} %copy.77), channel_id=1, replica_groups=mesh['ep'=16,'tp'=32] {'ep'}, dimensions={1} | all-to-all | bytes 524288 | tf_op jit(solution)/shard_map/all_to_all | solution.py:48
  26.4 0.7 copy.78
  27.1 0.0 all-gather.3.cloned.1.call-update
  27.1 0.0 all-gather.5.cloned.1.call-start
  27.2 98.1 %all-gather.3.cloned.1.call-done = bf16[2,512,4096]{2,1,0:T(8,128)(2,1)} async-done(((bf16[2,512,128]{2,1,0:T(8,128)(2,1)}), bf16[2,512,4096]{2,1,0:T(8,128)(2,1)}) %all-gather.3.cloned.1.call-update) | async-done | bytes 8388624 | tf_op jit(solution)/shard_map/all_gather | solution.py:51
  125.2 0.0 copy-start.1
  125.2 0.0 copy-start.3
  125.2 5.2 %fusion = f32[2,512]{1,0:T(2,128)S(1)} fusion(bf16[2,512,4096]{2,1,0:T(8,128)(2,1)} %all-gather.3.cloned.1.call-done), kind=kLoop, calls=%fused_computation.2 | loop fusion | flops 12581888 | bytes 8392704 | tf_op jit(solution)/shard_map/esn,esn->es/dot_general | solution.py:54
  130.5 0.0 copy-done.2
  130.5 0.5 copy-done.1
  131.0 0.0 copy-start.4
  131.0 2.6 %fusion.3 = f32[2,32,512]{2,1,0:T(8,128)S(1)} fusion(bf16[2,512,4096]{2,1,0:T(8,128)(2,1)S(1)} %copy-done.1, bf16[2,32,4096]{2,1,0:T(8,128)(2,1)S(1)} %copy-done.2, f32[2,512]{1,0:T(2,128)S(1)} %add_rsqrt_fusion), kind=kOutput, calls=%fused_computation.10 | convolution fusion | flops 268468224 | bytes 9048064 | tf_op jit(solution)/shard_map/efn,esn->efs/dot_general | solution.py:52
  133.6 0.0 copy-done.3
  133.7 0.0 copy-start.5
  133.7 3.2 %fusion.5 = bf16[2,32,512]{2,1,0:T(8,128)(2,1)} fusion(bf16[2,512,4096]{2,1,0:T(8,128)(2,1)S(1)} %copy-done.1, bf16[2,32,4096]{2,1,0:T(8,128)(2,1)S(1)} %copy-done.3, f32[2,32,512]{2,1,0:T(8,128)S(1)} %fusion.3, f32[2,512]{1,0:T(2,128)S(1)} %add_rsqrt_fusion), kind=kOutput, calls=%fused_computation.12 | convolution fusion | flops 268664832 | bytes 9113600 | tf_op jit(solution)/shard_map/efn,esn->efs/dot_general | solution.py:53
  136.9 0.0 all-gather.5.cloned.1.call-update
  136.9 0.1 reshape.209
  137.0 0.0 copy-done.4
  137.0 0.1 copy.82
  137.2 67.7 %all-gather.5.cloned.1.call-done = bf16[2,1024,512]{2,1,0:T(8,128)(2,1)} async-done(((bf16[2,32,512]{2,1,0:T(8,128)(2,1)}), bf16[2,1024,512]{2,1,0:T(8,128)(2,1)}) %all-gather.5.cloned.1.call-update) | async-done | bytes 2097168 | tf_op jit(solution)/shard_map/all_gather | solution.py:62
  204.9 0.0 copy-done
  204.9 2.5 convolution_convert_fusion
  207.4 0.7 copy.79
  208.1 6.5 %all-to-all-start.1 = ((bf16[2,16,32,128]{3,2,0,1:T(8,128)(2,1)}), bf16[2,16,32,128]{3,2,0,1:T(8,128)(2,1)S(1)}, u32[]{:S(2)}, u32[]{:S(2)}) async-start(bf16[2,16,32,128]{3,2,0,1:T(8,128)(2,1)} %copy.79), calls=%async_computation.1 | async-start | bytes 524288 | tf_op jit(solution)/shard_map/all_to_all | solution.py:66
  214.7 8.2 %all-to-all-done.1 = bf16[2,16,32,128]{3,2,0,1:T(8,128)(2,1)S(1)} async-done(((bf16[2,16,32,128]{3,2,0,1:T(8,128)(2,1)}), bf16[2,16,32,128]{3,2,0,1:T(8,128)(2,1)S(1)}, u32[]{:S(2)}, u32[]{:S(2)}) %all-to-all-start.1) | async-done | bytes 262176 | tf_op jit(solution)/shard_map/all_to_all | solution.py:66
  222.9 1.3 gather_fusion
  224.2 0.2 fusion.6
  224.5 0.1 multiply_reduce_fusion
  224.6 21.2 %all_to_all.17 = f32[32,1,128]{2,1,0:T(1,128)S(1)} all-to-all(f32[32,1,128]{2,1,0:T(1,128)S(1)} %broadcast_in_dim.2), channel_id=1, replica_groups=mesh['ep'=16,'tp'=32] {'tp'}, dimensions={0} | all-to-all | bytes 32768 | tf_op jit(solution)/shard_map/all_to_all | solution.py:16
  245.9 0.0 copy-done.5
  245.9 0.7 multiply_convert_fusion
  (11 shorter events, 0.2 us)
Async XLA Ops:
  6.5 198.4 %copy-start = (bf16[2,1024,128]{2,1,0:T(8,128)(2,1)S(1)}, bf16[2,1024,128]{2,1,0:T(8,128)(2,1)}, u32[]{:S(2)}) copy-start(bf16[2,1024,128]{2,1,0:T(8,128)(2,1)} %param.12) | copy-start | bytes 1572868
  6.5 124.0 %copy-start.2 = (bf16[2,32,4096]{2,1,0:T(8,128)(2,1)S(1)}, bf16[2,32,4096]{2,1,0:T(8,128)(2,1)}, u32[]{:S(2)}) copy-start(bf16[2,32,4096]{2,1,0:T(8,128)(2,1)} %param.10) | copy-start | bytes 1572868
  6.5 118.7 %all-gather.3.cloned.1.call-start = ((), (), s32[]{:S(2)}) async-start(), calls=%async_computation.3 | async-start | bytes 8650752 | tf_op jit(solution)/shard_map/all_gather | solution.py:51
  27.1 177.8 %all-gather.5.cloned.1.call-start = ((), (), s32[]{:S(2)}) async-start(), calls=%async_computation.4 | async-start | bytes 2162688 | tf_op jit(solution)/shard_map/all_gather | solution.py:62
  125.2 5.8 %copy-start.1 = (bf16[2,512,4096]{2,1,0:T(8,128)(2,1)S(1)}, bf16[2,512,4096]{2,1,0:T(8,128)(2,1)}, u32[]{:S(2)}) copy-start(bf16[2,512,4096]{2,1,0:T(8,128)(2,1)} %all-gather.3.cloned.1.call-done) | copy-start | bytes 25165828
  125.2 8.4 %copy-start.3 = (bf16[2,32,4096]{2,1,0:T(8,128)(2,1)S(1)}, bf16[2,32,4096]{2,1,0:T(8,128)(2,1)}, u32[]{:S(2)}) copy-start(bf16[2,32,4096]{2,1,0:T(8,128)(2,1)} %param.11) | copy-start | bytes 1572868
  131.0 6.0 %copy-start.4 = (f32[128,4]{0,1:T(4,128)S(1)}, f32[128,4]{0,1:T(4,128)}, u32[]{:S(2)}) copy-start(f32[128,4]{0,1:T(4,128)} %param.9) | copy-start | bytes 6148
  133.7 112.2 %copy-start.5 = (f32[128]{0:T(128)S(1)}, f32[128]{0:T(128)}, u32[]{:S(2)}) copy-start(f32[128]{0:T(128)} %param.13) | copy-start | bytes 1540
  208.1 14.7 %all-to-all-start.1 = ((bf16[2,16,32,128]{3,2,0,1:T(8,128)(2,1)}), bf16[2,16,32,128]{3,2,0,1:T(8,128)(2,1)S(1)}, u32[]{:S(2)}, u32[]{:S(2)}) async-start(bf16[2,16,32,128]{3,2,0,1:T(8,128)(2,1)} %copy.79), calls=%async_computation.1 | async-start | bytes 524288 | tf_op jit(solution)/shard_map/all_to_all | solution.py:66
Sparse Core Ops, SparseCore 0:
  27.2 97.9 all-gather.2
  137.0 67.7 all-gather.4
where the time goes:
time: 254 us; the launch traced here: 253 us
  waiting for transfers between devices  174 us (69%)
  blocking collectives  36.1 us (14%)
  between operations  13.5 us (5%)
  matrix products  9.35 us (4%)
  other arithmetic  8.73 us (3%)
  starting transfers between devices  6.57 us (3%)
  local copies, waits for them, and re-layouts  5.09 us (2%)
    all_gather x1, waiting for transfers between devices, body(): piece_cols = lax.all_gather(arrived, 'tp', axis=2, tiled=True)  98.1 us
    all_gather x1, waiting for transfers between devices, body(): lax.all_gather(hidden, 'tp', axis=1, tiled=True)  67.7 us
    all_to_all x1, blocking collectives, from_everyone(): lax.all_to_all(jnp.broadcast_to(value[None], (length, *value.shape)), axi...  21.2 us
    all_to_all x1, blocking collectives, body(): lax.all_to_all(outgoing, 'ep', split_axis=1, concat_axis=1, tiled=True)  14.9 us
    all_to_all x1, waiting for transfers between devices, body(): lax.all_to_all(expert_out.reshape(EXP_DEV, ep_count, slot_count, out_part...  8.16 us
    all_to_all x1, starting transfers between devices, body(): lax.all_to_all(expert_out.reshape(EXP_DEV, ep_count, slot_count, out_part...  6.53 us
    dot_general x1, other arithmetic, body(): jnp.einsum('esn,esn->es', piece_cols, piece_cols, preferred_element_type=...  5.23 us
  transfers between devices with their start and end apart: 3, of which 3 were waited for; matrix products, arithmetic and copies ran while one was open for 0% of the time, Pallas kernels for 0%

commit v1 on v0

v1 whole, which is shorter than its diff:
```python
import functools
import jax
import jax.numpy as jnp
from jax import lax
from jax.experimental import pallas as pl
from jax.experimental.pallas import tpu as pltpu
from jax.sharding import PartitionSpec as P

EXP_DEV = 2
CAP = 32
NORM_EPS = 1e-05
MESH = pl.DeviceIdType.MESH
F32 = jnp.float32
BF16 = jnp.bfloat16


def dot(a, b, dims):
    return lax.dot_general(a, b, (dims, ((), ())), preferred_element_type=F32)


def layer_kernel(
    n_ep, n_z, tok_ref, rt_ref, gw_ref, wg_ref, wu_ref, wd_ref, gain_ref, out_ref,
    outgoing, combine_w, x_all, w_all, d_all, acc, squares, h_all, o_acc, back, y_all, norm_all,
    w_sem, w_send, w_recv, d_send, d_recv, local_sem,
    x_send, x_recv, h_send, h_recv, r_send, r_recv, n_send, n_recv,
):
    ep = lax.axis_index("ep")
    tp = lax.axis_index("tp")
    z, c = tp // 2, tp % 2
    other = 1 - c
    partner = 2 * z + other
    above, below = (z + 1) % n_z, (z + n_z - 1) % n_z
    n_exp = EXP_DEV * n_ep
    n_tp = 2 * n_z
    tok_rows, width = tok_ref.shape
    half = n_z // 2
    rows = n_ep * CAP

    barrier = pltpu.get_barrier_semaphore()

    def greet(j, carry):
        p_to, c_to = (ep + j // 2) % n_ep, (c + j % 2) % 2
        pl.semaphore_signal(barrier, inc=1, device_id=(p_to, 2 * z + c_to), device_id_type=MESH)
        return carry

    lax.fori_loop(1, 2 * n_ep, greet, 0)
    pl.semaphore_signal(barrier, inc=1, device_id=(ep, 2 * above + c), device_id_type=MESH)
    pl.semaphore_signal(barrier, inc=1, device_id=(ep, 2 * below + c), device_id_type=MESH)

    own_w = [
        pltpu.make_async_copy(wg_ref.at[c], w_all.at[0, c], w_sem.at[0]),
        pltpu.make_async_copy(wu_ref.at[c], w_all.at[1, c], w_sem.at[1]),
        pltpu.make_async_copy(wd_ref.at[c], d_all.at[:, pl.ds(pl.multiple_of(c * width, width), width)], w_sem.at[2]),
    ]
    for copy in own_w:
        copy.start()

    rt = rt_ref[...]
    expert_ids = lax.broadcasted_iota(jnp.int32, (n_exp, tok_rows), 0)
    hits = [expert_ids == rt[k : k + 1, :] for k in range(rt.shape[0])]
    hit = functools.reduce(jnp.logical_or, hits)
    earlier = (
        lax.broadcasted_iota(jnp.int32, (tok_rows, tok_rows), 0)
        < lax.broadcasted_iota(jnp.int32, (tok_rows, tok_rows), 1)
    )
    rank = dot(
        jnp.where(hit, 1.0, 0.0).astype(BF16), jnp.where(earlier, 1.0, 0.0).astype(BF16), ((1,), (0,))
    )
    rank = jnp.where(hit, rank, -1.0)
    slot_ids = lax.broadcasted_iota(jnp.int32, (n_exp, CAP, tok_rows), 1).astype(F32)
    chosen = slot_ids == rank[:, None, :]
    select = jnp.where(chosen, 1.0, 0.0).astype(BF16).reshape(n_exp * CAP, tok_rows)
    outgoing[...] = dot(select, tok_ref[...], ((1,), (0,))).astype(BF16).reshape(n_exp, CAP, width)

    pl.semaphore_wait(barrier, 2 * n_ep - 1 + 2)

    def spread(j):
        p_to, c_to = (ep + j // 2) % n_ep, (c + j % 2) % 2
        return pltpu.make_async_remote_copy(
            src_ref=outgoing.at[2 * p_to + c_to],
            dst_ref=x_all.at[z, c, pl.ds(pl.multiple_of(ep * CAP, CAP), CAP)],
            send_sem=d_send.at[j],
            recv_sem=d_recv.at[j],
            device_id=(p_to, 2 * z + c_to),
            device_id_type=MESH,
        )

    def landed(j):
        p_from, c_from = (ep + n_ep - j // 2) % n_ep, (c + j % 2) % 2
        return pltpu.make_async_remote_copy(
            src_ref=outgoing.at[0],
            dst_ref=x_all.at[z, c_from, pl.ds(pl.multiple_of(p_from * CAP, CAP), CAP)],
            send_sem=d_send.at[j],
            recv_sem=d_recv.at[j],
            device_id=(p_from, 2 * z + c_from),
            device_id_type=MESH,
        )

    def each(lo, hi, act):
        def step(j, carry):
            act(j)
            return carry

        lax.fori_loop(lo, hi, step, 0)

    each(1, 2 * n_ep, lambda j: spread(j).start())
    own_x = pltpu.make_async_copy(
        outgoing.at[2 * ep + c], x_all.at[z, c, pl.ds(pl.multiple_of(ep * CAP, CAP), CAP)], local_sem.at[0]
    )
    own_x.start()

    pair_w = [
        pltpu.make_async_remote_copy(
            src_ref=src, dst_ref=dst, send_sem=w_send.at[i], recv_sem=w_recv.at[i],
            device_id=(ep, partner), device_id_type=MESH,
        )
        for i, (src, dst) in enumerate((
            (wg_ref.at[other], w_all.at[0, c]),
            (wu_ref.at[other], w_all.at[1, c]),
            (wd_ref.at[other], d_all.at[:, pl.ds(pl.multiple_of(c * width, width), width)]),
        ))
    ]
    pair_in = [
        pltpu.make_async_remote_copy(
            src_ref=src, dst_ref=dst, send_sem=w_send.at[i], recv_sem=w_recv.at[i],
            device_id=(ep, partner), device_id_type=MESH,
        )
        for i, (src, dst) in enumerate((
            (wg_ref.at[other], w_all.at[0, other]),
            (wu_ref.at[other], w_all.at[1, other]),
            (wd_ref.at[other], d_all.at[:, pl.ds(pl.multiple_of(other * width, width), width)]),
        ))
    ]
    for copy in pair_w:
        copy.start()

    gate_of = functools.reduce(
        jnp.add, [jnp.where(hits[k], gw_ref[k : k + 1, :], 0.0) for k in range(rt.shape[0])]
    )
    weight = jnp.where(chosen, gate_of[:, None, :], 0.0).reshape(n_exp * CAP, tok_rows).T
    weight_hi = weight.astype(BF16)
    combine_w[0] = weight_hi
    combine_w[1] = (weight - weight_hi.astype(F32)).astype(BF16)

    acc[...] = jnp.zeros_like(acc)
    squares[...] = jnp.zeros_like(squares)
    o_acc[...] = jnp.zeros_like(o_acc)

    def ring(buf, send, recv, use):
        def hop(way, s, ch):
            block = (z + n_z - s) % n_z if way == 0 else (z + s) % n_z
            to = above if way == 0 else below
            return pltpu.make_async_remote_copy(
                src_ref=buf.at[block, ch], dst_ref=buf.at[block, ch],
                send_sem=send.at[way, s, ch], recv_sem=recv.at[way, s, ch],
                device_id=(ep, 2 * to + c), device_id_type=MESH,
            )

        def came(way, s, ch):
            block = (z + n_z - s) % n_z if way == 0 else (z + s) % n_z
            return pltpu.make_async_remote_copy(
                src_ref=buf.at[block, ch], dst_ref=buf.at[block, ch],
                send_sem=send.at[way, s - 1, ch], recv_sem=recv.at[way, s - 1, ch],
                device_id=(ep, 2 * (below if way == 0 else above) + c), device_id_type=MESH,
            )

        order = ((0, 0), (1, 1), (0, 1), (1, 0))
        for way, ch in order:
            hop(way, 0, ch).start()
        use(z, 0)
        use(z, 1)

        def step(s):
            for way, ch in order:
                came(way, s, ch).wait_recv()
                hop(way, s, ch).start()
            for way, ch in order:
                use((z + n_z - s) % n_z if way == 0 else (z + s) % n_z, ch)

        each(1, half - 1, step)
        s = half - 1
        for way, ch in order:
            came(way, s, ch).wait_recv()
            if way == ch:
                hop(way, s, ch).start()
        for way, ch in order:
            use((z + n_z - s) % n_z if way == 0 else (z + s) % n_z, ch)
        for way in (0, 1):
            came(way, half, way).wait_recv()
            use((z + half) % n_z, way)

        def sent():
            def done(s):
                for way, ch in order:
                    hop(way, s, ch).wait_send()

            each(0, half - 1, done)
            for way in (0, 1):
                hop(way, half - 1, way).wait_send()

        return sent

    own_x.wait()
    each(1, 2 * n_ep, lambda j: landed(j).wait_recv())
    for copy in own_w:
        copy.wait()
    for copy in pair_in:
        copy.wait_recv()

    n_hid = 2 * w_all.shape[2]

    def project(block, ch):
        x = x_all[block, ch]
        column = pl.multiple_of((2 * block + ch) * width, width)
        w = w_all[:, :, :, pl.ds(column, width)].reshape(2 * n_hid, width)
        acc[...] += dot(w, x, ((1,), (1,)))
        x = x.astype(F32)
        squares[...] += x * x

    x_sent = ring(x_all, x_send, x_recv, project)

    features = n_tp * width
    square_sum = jnp.sum(squares[...].T, axis=0, keepdims=True)
    row_scale = lax.rsqrt(square_sum * (1.0 / features) + NORM_EPS)
    gate = acc[0:n_hid, :] * row_scale
    up = acc[n_hid : 2 * n_hid, :] * row_scale
    hidden = (gate / (1.0 + jnp.exp(-gate)) * up).astype(BF16)
    part = rows // 2
    for i in range(2):
        h_all[z, i] = hidden[:, i * part : (i + 1) * part]

    def down(block, ch):
        w = d_all[pl.ds(pl.multiple_of(block * n_hid, n_hid), n_hid), :]
        o_acc[ch] += dot(h_all[block, ch], w, ((0,), (0,)))

    h_sent = ring(h_all, h_send, h_recv, down)

    for i in range(2):
        for h in range(2):
            back[h, i * (n_ep // 2) : (i + 1) * (n_ep // 2)] = (
                o_acc[i, :, h * width : (h + 1) * width].astype(BF16).reshape(n_ep // 2, CAP, width)
            )

    def give(j):
        p_to, c_to = (ep + j // 2) % n_ep, (c + j % 2) % 2
        return pltpu.make_async_remote_copy(
            src_ref=back.at[c_to, p_to], dst_ref=y_all.at[2 * ep + c],
            send_sem=r_send.at[j], recv_sem=r_recv.at[j],
            device_id=(p_to, 2 * z + c_to), device_id_type=MESH,
        )

    def got(j):
        p_from, c_from = (ep + n_ep - j // 2) % n_ep, (c + j % 2) % 2
        return pltpu.make_async_remote_copy(
            src_ref=back.at[0, 0], dst_ref=y_all.at[2 * p_from + c_from],
            send_sem=r_send.at[j], recv_sem=r_recv.at[j],
            device_id=(p_from, 2 * z + c_from), device_id_type=MESH,
        )

    each(1, 2 * n_ep, lambda j: give(j).start())
    own_y = pltpu.make_async_copy(back.at[c, ep], y_all.at[2 * ep + c], local_sem.at[1])
    own_y.start()

    each(1, 2 * n_ep, lambda j: spread(j).wait_send())
    for copy in pair_w:
        copy.wait_send()
    x_sent()
    h_sent()

    own_y.wait()
    each(1, 2 * n_ep, lambda j: got(j).wait_recv())
    y = y_all[...].reshape(n_exp * CAP, width)
    combined = dot(combine_w[0], y, ((1,), (0,))) + dot(combine_w[1], y, ((1,), (0,)))
    norm_all[tp] = jnp.sum((combined * combined).T, axis=0, keepdims=True)

    def tell(j):
        return pltpu.make_async_remote_copy(
            src_ref=norm_all.at[tp], dst_ref=norm_all.at[tp],
            send_sem=n_send.at[j], recv_sem=n_recv.at[j],
            device_id=(ep, (tp + j) % n_tp), device_id_type=MESH,
        )

    def told(j):
        t_from = (tp + n_tp - j) % n_tp
        return pltpu.make_async_remote_copy(
            src_ref=norm_all.at[t_from], dst_ref=norm_all.at[t_from],
            send_sem=n_send.at[j], recv_sem=n_recv.at[j],
            device_id=(ep, t_from), device_id_type=MESH,
        )

    each(1, n_tp, lambda j: tell(j).start())
    scaled = combined * gain_ref[...]
    each(1, 2 * n_ep, lambda j: give(j).wait_send())
    each(1, n_tp, lambda j: told(j).wait_recv())
    total = jnp.sum(norm_all[...], axis=0)
    final_scale = lax.rsqrt(total * (1.0 / features) + NORM_EPS)
    final_scale = jnp.broadcast_to(final_scale, (tok_rows, tok_rows)).T
    out_ref[...] = (scaled * final_scale[:, :width]).astype(out_ref.dtype)
    each(1, n_tp, lambda j: tell(j).wait_send())


def body(tokens, routing, gate_weights, w_gate, w_up, w_down, out_gain):
    n_ep = lax.axis_size("ep")
    n_tp = lax.axis_size("tp")
    n_z = n_tp // 2
    tok_rows, width = tokens.shape
    n_exp = EXP_DEV * n_ep
    rows = n_ep * CAP
    hid, model = w_gate.shape[1], w_gate.shape[2]
    full = w_down.shape[1]
    vmem = pl.BlockSpec(memory_space=pltpu.VMEM)
    hbm = pl.BlockSpec(memory_space=pl.ANY)
    dma = pltpu.SemaphoreType.DMA
    return pl.pallas_call(
        functools.partial(layer_kernel, n_ep, n_z),
        out_shape=jax.ShapeDtypeStruct((tok_rows, width), BF16),
        in_specs=[vmem, vmem, vmem, hbm, hbm, hbm, vmem],
        out_specs=vmem,
        scratch_shapes=[
            pltpu.VMEM((n_exp, CAP, width), BF16),
            pltpu.VMEM((2, tok_rows, n_exp * CAP), BF16),
            pltpu.VMEM((n_z, 2, rows, width), BF16),
            pltpu.VMEM((2, 2, hid, model), BF16),
            pltpu.VMEM((full, 2 * width), BF16),
            pltpu.VMEM((4 * hid, rows), F32),
            pltpu.VMEM((rows, width), F32),
            pltpu.VMEM((n_z, 2, 2 * hid, rows // 2), BF16),
            pltpu.VMEM((2, rows // 2, 2 * width), F32),
            pltpu.VMEM((2, n_ep, CAP, width), BF16),
            pltpu.VMEM((n_exp, CAP, width), BF16),
            pltpu.VMEM((n_tp, 1, tok_rows), F32),
            dma((3,)), dma((3,)), dma((3,)), dma((2 * n_ep,)), dma((2 * n_ep,)), dma((2,)),
            dma((2, n_z // 2, 2)), dma((2, n_z // 2, 2)),
            dma((2, n_z // 2, 2)), dma((2, n_z // 2, 2)),
            dma((2 * n_ep,)), dma((2 * n_ep,)), dma((n_tp,)), dma((n_tp,)),
        ],
        compiler_params=pltpu.CompilerParams(collective_id=0, has_side_effects=True),
        name="expert_layer",
    )(tokens, routing.T, gate_weights.T, w_gate, w_up, w_down, out_gain.reshape(1, -1))


def solution(mesh):
    placed = (
        P("ep", "tp"),
        P("ep", None),
        P("ep", None),
        P("ep", "tp", None),
        P("ep", "tp", None),
        P("ep", None, "tp"),
        P("tp"),
    )
    return jax.shard_map(body, mesh=mesh, in_specs=placed, out_specs=P("ep", "tp"), check_vma=False)
```

time: 254 us -> 112 us (0.44)
  waiting for transfers between devices: 174 us -> 0 us
  Pallas kernels: 0 us -> 110 us
  blocking collectives: 36.1 us -> 0 us
  between operations: 13.5 us -> 0.01 us
  matrix products: 9.35 us -> 0 us
  other arithmetic: 8.73 us -> 0 us
  starting transfers between devices: 6.57 us -> 0 us
  local copies, waits for them, and re-layouts: 5.09 us -> 1.38 us
    all_gather x2 -> x0, waiting for transfers between devices: 166 us -> none  [the longest x1 98.1 us: body(): piece_cols = lax.all_gather(arrived, 'tp', axis=2, tiled=True)]
    pallas_call x0 -> x1, Pallas kernels: none -> 110 us  [body(): pl.pallas_call(functools.partial(layer_kernel, n_ep, n_z), out_shape=jax....]
    all_to_all x2 -> x0, blocking collectives: 36.1 us -> none  [the longest x1 21.2 us: from_everyone(): lax.all_to_all(jnp.broadcast_to(value[None], (length, *value.shape)), axi...]
    dot_general x4 -> x0, matrix products: 9.35 us -> none  [the longest x1 3.24 us: body(): jnp.einsum('efn,esn->efs', w_up, piece_cols, preferred_element_type=jnp.f...]
    all_to_all x1 -> x0, waiting for transfers between devices: 8.16 us -> none  [body(): lax.all_to_all(expert_out.reshape(EXP_DEV, ep_count, slot_count, out_part...]
    all_to_all x1 -> x0, starting transfers between devices: 6.53 us -> none  [body(): lax.all_to_all(expert_out.reshape(EXP_DEV, ep_count, slot_count, out_part...]
    dot_general x1 -> x0, other arithmetic: 5.23 us -> none  [body(): jnp.einsum('esn,esn->es', piece_cols, piece_cols, preferred_element_type=...]
  transfers between devices with their start and end apart: 3 -> 0, of which waited for: 3 -> 0; matrix products, arithmetic and copies ran while one was open for 0% -> 0% of each run, Pallas kernels for 0% -> 0%
where the time goes in v1:
time: 112 us; the launch traced here: 111 us
  Pallas kernels  110 us (98%)
  local copies, waits for them, and re-layouts  1.38 us (1%)
    pallas_call x1, Pallas kernels, body(): pl.pallas_call(functools.partial(layer_kernel, n_ep, n_z), out_shape=jax....  110 us

profile of v1, /device:TPU:1, one launch (start us, length us, event | category | flops | bytes accessed | tf_op | source)
XLA Modules:
  0.0 111.4 jit_solution(3569158049509999523)
XLA Ops:
  0.0 110.0 %expert_layer.1 = bf16[128,128]{1,0:T(8,128)(2,1)} custom-call(bf16[128,128]{1,0:T(8,128)(2,1)} %tok_ref.1, s32[4,128]{1,0:T(4,128)} %bitcast.3, f32[4,128]{1,0:T(4,128)} %bitcast.4, bf16[2,32,4096]{2,1,0:T(8,128)(2,1)} %wg_ref.1, bf16[2,32,4096]{2,1,0:T(8,128)(2,1)} %wu_ref.1, bf16[2,1024,128]{2,1,0:T(8,128)(2,1)} %wd_ref.1, f32[1,128]{1,0:T(1,128)} %bitcast.5), custom_call_target="tpu_custom_call" | custom-call | tf_op jit(solution)/shard_map/expert_layer/pallas_call | solution.py:314
  110.0 1.4 %copy.9 = bf16[128,128]{1,0:T(8,128)(2,1)} copy(bf16[128,128]{1,0:T(8,128)(2,1)} %expert_layer.1) | data formatting | bytes 65536

commit v2 on v1

v2 whole, which is shorter than its diff:
```python
import functools
import math
import jax
import jax.numpy as jnp
from jax import lax
from jax.experimental import pallas as pl
from jax.experimental.pallas import tpu as pltpu
from jax.sharding import PartitionSpec as P

EXP_DEV = 2
CAP = 32
NORM_EPS = 1e-05
MESH = pl.DeviceIdType.MESH
F32 = jnp.float32
BF16 = jnp.bfloat16


def dot(a, b, dims):
    return lax.dot_general(a, b, (dims, ((), ())), preferred_element_type=F32)


def layer_kernel(
    side, n_z, tok_ref, rt_ref, gw_ref, wg_ref, wu_ref, wd_ref, gain_ref, out_ref,
    t_all, routes, gates, gain, select, staged, combine_w, x_all, w_all, d_all, acc, squares,
    h_all, o_acc, back, y_all, norm_all,
    in_sem, w_sem, w_send, w_recv, m_send, m_recv, q_send, q_recv, t_send, t_recv, p_send, p_recv,
    h_send, h_recv, r_send, r_recv, n_send, n_recv, local_sem,
):
    ep = lax.axis_index("ep")
    tp = lax.axis_index("tp")
    z, c = tp // 2, tp % 2
    y, x = ep // side, ep % side
    other = 1 - c
    partner = 2 * z + other
    above, below = (z + 1) % n_z, (z + n_z - 1) % n_z
    n_ep = side * side
    n_exp = EXP_DEV * n_ep
    n_tp = 2 * n_z
    width = tok_ref.shape[1]
    tok_rows = tok_ref.shape[0]
    half = n_z // 2
    rows = n_ep * CAP

    g_own = other * y + c * x
    d_own = other * x + c * y

    def g_ep(g):
        return other * (g * side + x) + c * (y * side + g)

    def d_ep(d):
        return other * (y * side + d) + c * (d * side + x)

    def each(lo, hi, act):
        def step(j, carry):
            act(j)
            return carry

        lax.fori_loop(lo, hi, step, 0)

    barrier = pltpu.get_barrier_semaphore()

    def greet(p_to, t_to):
        pl.semaphore_signal(barrier, inc=1, device_id=(p_to, t_to), device_id_type=MESH)

    for k in range(1, side):
        greet(g_ep((g_own + k) % side), tp)
        greet(y * side + (x + k) % side, 2 * z)
        greet(((y + k) % side) * side + x, 2 * z + 1)
    greet(ep, partner)
    greet(ep, 2 * above + c)
    greet(ep, 2 * below + c)
    n_greet = 3 * (side - 1) + 3

    own_in = [
        pltpu.make_async_copy(tok_ref, t_all.at[z, g_own // 2, g_own % 2], in_sem.at[0]),
        pltpu.make_async_copy(rt_ref, routes.at[g_own], in_sem.at[1]),
        pltpu.make_async_copy(gw_ref, gates, in_sem.at[2]),
        pltpu.make_async_copy(gain_ref, gain, in_sem.at[3]),
    ]
    own_w = [
        pltpu.make_async_copy(wg_ref.at[c], w_all.at[0, c], w_sem.at[0]),
        pltpu.make_async_copy(wu_ref.at[c], w_all.at[1, c], w_sem.at[1]),
        pltpu.make_async_copy(wd_ref.at[c], d_all.at[:, pl.ds(pl.multiple_of(c * width, width), width)], w_sem.at[2]),
    ]
    for copy in own_in:
        copy.start()
    for copy in own_w:
        copy.start()
    own_in[0].wait()
    own_in[1].wait()
    pl.semaphore_wait(barrier, n_greet)

    def share(k):
        to = (g_ep((g_own + k) % side), tp)
        mine = t_all.at[z, g_own // 2, g_own % 2]
        return [
            pltpu.make_async_remote_copy(
                src_ref=mine, dst_ref=mine, send_sem=m_send.at[k - 1], recv_sem=m_recv.at[k - 1],
                device_id=to, device_id_type=MESH,
            ),
            pltpu.make_async_remote_copy(
                src_ref=routes.at[g_own], dst_ref=routes.at[g_own],
                send_sem=q_send.at[k - 1], recv_sem=q_recv.at[k - 1],
                device_id=to, device_id_type=MESH,
            ),
        ]

    def shared(k):
        g = (g_own + side - k) % side
        theirs = t_all.at[z, g // 2, g % 2]
        return [
            pltpu.make_async_remote_copy(
                src_ref=theirs, dst_ref=theirs, send_sem=m_send.at[k - 1], recv_sem=m_recv.at[k - 1],
                device_id=(g_ep(g), tp), device_id_type=MESH,
            ),
            pltpu.make_async_remote_copy(
                src_ref=routes.at[g], dst_ref=routes.at[g],
                send_sem=q_send.at[k - 1], recv_sem=q_recv.at[k - 1],
                device_id=(g_ep(g), tp), device_id_type=MESH,
            ),
        ]

    for k in (2, 1, 3):
        for copy in share(k):
            copy.start()

    def pair(i, src, dst):
        return pltpu.make_async_remote_copy(
            src_ref=src, dst_ref=dst, send_sem=w_send.at[i], recv_sem=w_recv.at[i],
            device_id=(ep, partner), device_id_type=MESH,
        )

    def d_part(k):
        return d_all.at[:, pl.ds(pl.multiple_of(k * width, width), width)]

    pair_w = [
        pair(0, wg_ref.at[other], w_all.at[0, c]),
        pair(1, wu_ref.at[other], w_all.at[1, c]),
        pair(2, wd_ref.at[other], d_part(c)),
    ]
    pair_in = [
        pair(0, wg_ref.at[other], w_all.at[0, other]),
        pair(1, wu_ref.at[other], w_all.at[1, other]),
        pair(2, wd_ref.at[other], d_part(other)),
    ]
    for copy in pair_w:
        copy.start()

    acc[...] = jnp.zeros_like(acc)
    squares[...] = jnp.zeros_like(squares)
    o_acc[...] = jnp.zeros_like(o_acc)

    earlier = jnp.where(
        lax.broadcasted_iota(jnp.int32, (tok_rows, tok_rows), 0)
        < lax.broadcasted_iota(jnp.int32, (tok_rows, tok_rows), 1),
        1.0, 0.0,
    ).astype(BF16)

    def slots(hit):
        rank = dot(jnp.where(hit, 1.0, 0.0).astype(BF16), earlier, ((1,), (0,)))
        rank = jnp.where(hit, rank, -1.0)
        slot_ids = lax.broadcasted_iota(jnp.int32, (hit.shape[0], CAP, tok_rows), 1).astype(F32)
        return slot_ids == rank[:, None, :]

    def hits_of(ids, route):
        return [ids == route[k : k + 1, :] for k in range(route.shape[0])]

    order = ((0, 0), (1, 1), (0, 1), (1, 0))

    def block_of(way, s):
        return (z + n_z - s) % n_z if way == 0 else (z + s) % n_z

    def hop(buf, send, recv, way, s, ch):
        block = block_of(way, s)
        return pltpu.make_async_remote_copy(
            src_ref=buf.at[block, ch], dst_ref=buf.at[block, ch],
            send_sem=send.at[way, s, ch], recv_sem=recv.at[way, s, ch],
            device_id=(ep, 2 * (above if way == 0 else below) + c), device_id_type=MESH,
        )

    def came(buf, send, recv, way, s, ch):
        block = block_of(way, s)
        return pltpu.make_async_remote_copy(
            src_ref=buf.at[block, ch], dst_ref=buf.at[block, ch],
            send_sem=send.at[way, s - 1, ch], recv_sem=recv.at[way, s - 1, ch],
            device_id=(ep, 2 * (below if way == 0 else above) + c), device_id_type=MESH,
        )

    def ring_start(ring):
        for way, ch in order:
            hop(*ring, way, 0, ch).start()

    def ring_step(ring, s):
        for way, ch in order:
            came(*ring, way, s, ch).wait_recv()
            hop(*ring, way, s, ch).start()

    def ring_late(ring):
        s = half - 1
        for way, ch in order:
            came(*ring, way, s, ch).wait_recv()
            if way == ch:
                hop(*ring, way, s, ch).start()

    def ring_sent(ring):
        def done(s):
            for way, ch in order:
                hop(*ring, way, s, ch).wait_send()

        each(0, half - 1, done)
        for way in (0, 1):
            hop(*ring, way, half - 1, way).wait_send()

    t_ring = (t_all, t_send, t_recv)
    h_ring = (h_all, h_send, h_recv)

    for k in (1, 3, 2):
        for copy in shared(k):
            copy.wait_recv()
    ring_start(t_ring)

    line = lax.broadcasted_iota(jnp.int32, (2 * side, tok_rows), 0)
    line = 2 * d_ep(line // 2) + line % 2
    line_hits = [functools.reduce(jnp.logical_or, hits_of(line, routes[g])) for g in range(side)]
    chosen = slots(jnp.concatenate([jnp.where(h, 1.0, 0.0) for h in line_hits], axis=0) > 0.5)
    select[...] = jnp.where(chosen, 1.0, 0.0).astype(BF16).reshape(side, 2 * side * CAP, tok_rows)

    def piece(block, d, e):
        return pltpu.make_async_remote_copy(
            src_ref=staged.at[block, 2 * d + e], dst_ref=x_all.at[block, c, d_own],
            send_sem=p_send.at[block, 2 * d + e], recv_sem=p_recv.at[block, c, d_own],
            device_id=(d_ep(d), 2 * z + e), device_id_type=MESH,
        )

    def own_piece(block):
        return pltpu.make_async_copy(
            staged.at[block, 2 * d_own + c], x_all.at[block, c, d_own], p_recv.at[block, c, d_own]
        )

    def expand(block):
        for g in range(side):
            picked = dot(select[g], t_all[block, g // 2, g % 2], ((1,), (0,))).astype(BF16)
            staged[block, :, g] = picked.reshape(2 * side, CAP, width)
        for k in (2, 1, 3):
            for e in range(2):
                piece(block, (d_own + k) % side, e).start()
        piece(block, d_own, other).start()
        own_piece(block).start()

    def pieces_sent(block):
        for k in range(1, side):
            for e in range(2):
                piece(block, (d_own + k) % side, e).wait_send()
        piece(block, d_own, other).wait_send()

    n_hid = 2 * w_all.shape[2]

    def project(block):
        for ch in range(2):
            for i in range(side):
                pltpu.make_async_copy(
                    staged.at[block, 0], x_all.at[block, ch, i], p_recv.at[block, ch, i]
                ).wait()
            parts = [
                x_all[block, ch, i, j] if ch == 0 else x_all[block, ch, j, i]
                for i in range(side) for j in range(side)
            ]
            data = jnp.concatenate(parts, axis=0)
            column = pl.multiple_of((2 * block + ch) * width, width)
            w = w_all[:, :, :, pl.ds(column, width)].reshape(2 * n_hid, width)
            acc[...] += dot(w, data, ((1,), (1,)))
            data = data.astype(F32)
            squares[...] += data * data

    expand(z)
    for copy in own_w:
        copy.wait()
    for copy in pair_in:
        copy.wait_recv()

    def middle(s):
        ring_step(t_ring, s)
        for way in range(2):
            expand(block_of(way, s))

        @pl.when(s >= 3)
        def _():
            for way in range(2):
                project(block_of(way, s - 2))

    each(1, half - 1, middle)
    ring_late(t_ring)
    for way in range(2):
        expand(block_of(way, half - 1))
    for way in range(2):
        project(block_of(way, half - 3))
    for way in range(2):
        came(*t_ring, way, half, way).wait_recv()
    expand(block_of(0, half))
    project(z)
    for way in range(2):
        project(block_of(way, half - 2))

    own_in[2].wait()
    own_in[3].wait()
    all_ids = lax.broadcasted_iota(jnp.int32, (n_exp, tok_rows), 0)
    hits = hits_of(all_ids, routes[g_own])
    gate_of = functools.reduce(jnp.add, [jnp.where(h, gates[k : k + 1, :], 0.0) for k, h in enumerate(hits)])
    weight = jnp.where(slots(functools.reduce(jnp.logical_or, hits)), gate_of[:, None, :], 0.0)
    weight = weight.reshape(n_exp * CAP, tok_rows).T
    weight_hi = weight.astype(BF16)
    combine_w[0] = weight_hi
    combine_w[1] = (weight - weight_hi.astype(F32)).astype(BF16)

    for way in range(2):
        project(block_of(way, half - 1))
    project(block_of(0, half))

    features = n_tp * width
    square_sum = jnp.sum(squares[...].T, axis=0, keepdims=True)
    row_scale = lax.rsqrt(square_sum * (1.0 / features) + NORM_EPS)
    gate = acc[0:n_hid, :] * row_scale
    up = acc[n_hid : 2 * n_hid, :] * row_scale
    hidden = (gate / (1.0 + jnp.exp(-gate)) * up).astype(BF16)
    part = rows // 2
    for i in range(2):
        h_all[z, i] = hidden[:, i * part : (i + 1) * part]

    def down(block, ch):
        w = d_all[pl.ds(pl.multiple_of(block * n_hid, n_hid), n_hid), :]
        o_acc[ch] += dot(h_all[block, ch], w, ((0,), (0,)))

    ring_start(h_ring)
    for ch in range(2):
        down(z, ch)

    def h_middle(s):
        ring_step(h_ring, s)
        for way, ch in order:
            down(block_of(way, s), ch)

    each(1, half - 1, h_middle)
    ring_late(h_ring)
    for way, ch in order:
        down(block_of(way, half - 1), ch)
    for way in range(2):
        came(*h_ring, way, half, way).wait_recv()
        down(block_of(way, half), way)

    s_half = side // 2
    for i in range(2):
        for h in range(2):
            back[h, i * s_half : (i + 1) * s_half] = (
                o_acc[i, :, h * width : (h + 1) * width].astype(BF16).reshape(s_half, side, CAP, width)
            )

    def give(j):
        p_to, c_to = (ep + j // 2) % n_ep, (c + j % 2) % 2
        return pltpu.make_async_remote_copy(
            src_ref=back.at[c_to, p_to % side, p_to // side], dst_ref=y_all.at[2 * ep + c],
            send_sem=r_send.at[j], recv_sem=r_recv.at[j],
            device_id=(p_to, 2 * z + c_to), device_id_type=MESH,
        )

    def got(j):
        p_from, c_from = (ep + n_ep - j // 2) % n_ep, (c + j % 2) % 2
        return pltpu.make_async_remote_copy(
            src_ref=back.at[0, 0, 0], dst_ref=y_all.at[2 * p_from + c_from],
            send_sem=r_send.at[j], recv_sem=r_recv.at[j],
            device_id=(p_from, 2 * z + c_from), device_id_type=MESH,
        )

    each(1, 2 * n_ep, lambda j: give(j).start())
    own_y = pltpu.make_async_copy(back.at[c, ep % side, ep // side], y_all.at[2 * ep + c], local_sem.at[0])
    own_y.start()

    for k in range(1, side):
        for copy in share(k):
            copy.wait_send()
    for copy in pair_w:
        copy.wait_send()
    ring_sent(t_ring)
    each(0, n_z, pieces_sent)
    ring_sent(h_ring)

    own_y.wait()
    each(1, 2 * n_ep, lambda j: got(j).wait_recv())
    returned = y_all[...].reshape(n_exp * CAP, width)
    combined = dot(combine_w[0], returned, ((1,), (0,))) + dot(combine_w[1], returned, ((1,), (0,)))
    norm_all[tp] = jnp.sum((combined * combined).T, axis=0, keepdims=True)

    def tell(j):
        return pltpu.make_async_remote_copy(
            src_ref=norm_all.at[tp], dst_ref=norm_all.at[tp],
            send_sem=n_send.at[j], recv_sem=n_recv.at[j],
            device_id=(ep, (tp + j) % n_tp), device_id_type=MESH,
        )

    def told(j):
        t_from = (tp + n_tp - j) % n_tp
        return pltpu.make_async_remote_copy(
            src_ref=norm_all.at[t_from], dst_ref=norm_all.at[t_from],
            send_sem=n_send.at[j], recv_sem=n_recv.at[j],
            device_id=(ep, t_from), device_id_type=MESH,
        )

    each(1, n_tp, lambda j: tell(j).start())
    scaled = combined * gain[...]
    each(1, 2 * n_ep, lambda j: give(j).wait_send())
    each(1, n_tp, lambda j: told(j).wait_recv())
    total = jnp.sum(norm_all[...], axis=0)
    final_scale = lax.rsqrt(total * (1.0 / features) + NORM_EPS)
    final_scale = jnp.broadcast_to(final_scale, (tok_rows, tok_rows)).T
    out_ref[...] = (scaled * final_scale[:, :width]).astype(out_ref.dtype)
    each(1, n_tp, lambda j: tell(j).wait_send())


def body(tokens, routing, gate_weights, w_gate, w_up, w_down, out_gain):
    n_ep = lax.axis_size("ep")
    n_tp = lax.axis_size("tp")
    side = math.isqrt(n_ep)
    n_z = n_tp // 2
    tok_rows, width = tokens.shape
    top = routing.shape[1]
    n_exp = EXP_DEV * n_ep
    rows = n_ep * CAP
    hid, model = w_gate.shape[1], w_gate.shape[2]
    full = w_down.shape[1]
    hbm = pl.BlockSpec(memory_space=pl.ANY)
    dma = pltpu.SemaphoreType.DMA
    ring = (2, n_z // 2, 2)
    return pl.pallas_call(
        functools.partial(layer_kernel, side, n_z),
        out_shape=jax.ShapeDtypeStruct((tok_rows, width), BF16),
        in_specs=[hbm] * 7,
        out_specs=pl.BlockSpec(memory_space=pltpu.VMEM),
        scratch_shapes=[
            pltpu.VMEM((n_z, side // 2, 2, tok_rows, width), BF16),
            pltpu.VMEM((side, top, tok_rows), jnp.int32),
            pltpu.VMEM((top, tok_rows), F32),
            pltpu.VMEM((1, width), F32),
            pltpu.VMEM((side, 2 * side * CAP, tok_rows), BF16),
            pltpu.VMEM((n_z, 2 * side, side, CAP, width), BF16),
            pltpu.VMEM((2, tok_rows, n_exp * CAP), BF16),
            pltpu.VMEM((n_z, 2, side, side, CAP, width), BF16),
            pltpu.VMEM((2, 2, hid, model), BF16),
            pltpu.VMEM((full, 2 * width), BF16),
            pltpu.VMEM((4 * hid, rows), F32),
            pltpu.VMEM((rows, width), F32),
            pltpu.VMEM((n_z, 2, 2 * hid, rows // 2), BF16),
            pltpu.VMEM((2, rows // 2, 2 * width), F32),
            pltpu.VMEM((2, side, side, CAP, width), BF16),
            pltpu.VMEM((n_exp, CAP, width), BF16),
            pltpu.VMEM((n_tp, 1, tok_rows), F32),
            dma((4,)), dma((3,)), dma((3,)), dma((3,)),
            dma((side - 1,)), dma((side - 1,)), dma((side - 1,)), dma((side - 1,)),
            dma(ring), dma(ring), dma((n_z, 2 * side)), dma((n_z, 2, side)),
            dma(ring), dma(ring), dma((2 * n_ep,)), dma((2 * n_ep,)), dma((n_tp,)), dma((n_tp,)), dma((1,)),
        ],
        compiler_params=pltpu.CompilerParams(collective_id=0, has_side_effects=True),
        name="expert_layer",
    )(tokens, routing.T, gate_weights.T, w_gate, w_up, w_down, out_gain.reshape(1, -1))


def solution(mesh):
    placed = (
        P("ep", "tp"),
        P("ep", None),
        P("ep", None),
        P("ep", "tp", None),
        P("ep", "tp", None),
        P("ep", None, "tp"),
        P("tp"),
    )
    return jax.shard_map(body, mesh=mesh, in_specs=placed, out_specs=P("ep", "tp"), check_vma=False)
```

time: 112 us -> 99.4 us (0.89)
  Pallas kernels: 110 us -> 97.8 us
    pallas_call x1, Pallas kernels: 110 us -> 97.8 us  [body(): pl.pallas_call(functools.partial(layer_kernel, side, n_z), out_shape=jax....]
where the time goes in v2:
time: 99.4 us; the launch traced here: 99.2 us
  Pallas kernels  97.8 us (98%)
  local copies, waits for them, and re-layouts  1.38 us (1%)
    pallas_call x1, Pallas kernels, body(): pl.pallas_call(functools.partial(layer_kernel, side, n_z), out_shape=jax....  97.8 us

profile of v2, /device:TPU:1, one launch (start us, length us, event | category | flops | bytes accessed | tf_op | source)
XLA Modules:
  0.0 99.2 jit_solution(1565205818585196387)
XLA Ops:
  0.0 97.8 %expert_layer.1 = bf16[128,128]{1,0:T(8,128)(2,1)} custom-call(bf16[128,128]{1,0:T(8,128)(2,1)} %tok_ref.1, s32[4,128]{1,0:T(4,128)} %bitcast.3, f32[4,128]{1,0:T(4,128)} %bitcast.4, bf16[2,32,4096]{2,1,0:T(8,128)(2,1)} %wg_ref.1, bf16[2,32,4096]{2,1,0:T(8,128)(2,1)} %wu_ref.1, bf16[2,1024,128]{2,1,0:T(8,128)(2,1)} %wd_ref.1, f32[1,128]{1,0:T(1,128)} %bitcast.5), custom_call_target="tpu_custom_call" | custom-call | tf_op jit(solution)/shard_map/expert_layer/pallas_call | solution.py:432
  97.8 1.4 %copy.9 = bf16[128,128]{1,0:T(8,128)(2,1)} copy(bf16[128,128]{1,0:T(8,128)(2,1)} %expert_layer.1) | data formatting | bytes 65536
